TPU v7x, 32 devices: a whole 2x2x4 slice. The times are simulated.
32 devices in a mesh: grp: 2 (over y), sp: 4 (over z), tp: 4 (over x, core).
Axes of the slice: x: 2, y: 2, z: 4, core: 2. Of those that a mesh axis runs over, the one named last changes fastest.
Arguments:
- stream: bfloat16 [1024, 2048], P(('grp', 'sp')), parts along dimension 0, may hold values from -40 to 40
- queries: bfloat16 [1024, 1024], P(('grp', 'sp'), 'tp'), parts along dimension 0, may hold values from -6 to 6
- key_matrix: bfloat16 [1024, 1024], P(('grp', 'sp'), 'tp'), parts along dimension 0, may hold values from -6 to 6
- value_matrix: bfloat16 [1024, 2048], P(('grp', 'sp'), 'tp'), parts along dimension 0, may hold values from -6 to 6
- output_gate_logits: bfloat16 [1024, 2048], P(('grp', 'sp'), 'tp'), parts along dimension 0, may hold values from -6 to 6
- forgetting_raw_score: float32 [1024, 1024], P(('grp', 'sp'), 'tp'), parts along dimension 0, may hold values from -2 to 12
- additional_forgetting_rate: float32 [1024, 1024], P(('grp', 'sp'), 'tp'), parts along dimension 0, may hold values from -0.7 to 0
- head_norm_gain: float32 [2048], P('tp'), may hold values from 0.1 to 1.9
- output_weight: bfloat16 [2048, 2048], P('tp'), may hold values from -0.125 to 0.125
- feedforward_norm_gain: bfloat16 [2048], replicated, may hold values from 0.099609375 to 1.8984375
- gate_weight: bfloat16 [2048, 5632], P('sp', 'tp'), may hold values from -0.125 to 0.125
- up_weight: bfloat16 [2048, 5632], P('sp', 'tp'), may hold values from -0.125 to 0.125
- down_weight: bfloat16 [5632, 2048], P('tp', 'sp'), may hold values from -0.078125 to 0.078125
Outputs:
- layer_out: bfloat16 [1024, 2048], P(('grp', 'sp'), 'tp'), parts along dimension 0
There are 2 independent parts, one for each index of `grp`. A program takes and returns all parts, laid end to end along the dimension named above; an argument that names none is the same for every part. Nothing has to cross between parts.
All inputs are finite; a program needn't handle non-finite values.
Results may differ from a plain program's by a relative error of at most 0.013.
Values may be sent and summed in bfloat16 or wider, within the bound.
A program may use at most 128 MiB of HBM per device.

v0:
```python
import jax
import jax.numpy as jnp
from jax import lax
from jax.sharding import PartitionSpec as P

HK = 256
HV = 512
BLOCK = 64
epsilon = 1e-06
sigmoid_sharpness = 16.0
highest = lax.Precision.HIGHEST


def carried_in(value, axis, join, neutral):
    place = lax.axis_index(axis)
    gathered = jax.tree.map(
        lambda a, kind: lax.all_gather(a.astype(kind), axis), value, (jnp.bfloat16, jnp.bfloat16)
    )
    state = jax.tree.map(lambda a, e: jnp.zeros_like(a) + jnp.asarray(e, a.dtype), value, neutral)

    def one(turn, state):
        return join(
            state,
            jax.tree.map(
                lambda a, own: lax.dynamic_index_in_dim(a, turn, 0, False).astype(own.dtype),
                gathered,
                value,
            ),
        )

    return lax.fori_loop(0, place, one, state)


def split_heads(tensor, blocks, count, depth):
    return tensor.astype(jnp.float32).reshape(blocks, BLOCK, count, depth).transpose(2, 0, 1, 3)


def combine(earlier, later):
    return (earlier[0] * later[0], later[0][:, :, None] * earlier[1] + later[1])


def local(
    stream,
    queries,
    key_matrix,
    value_matrix,
    output_gate_logits,
    forgetting_raw_score,
    additional_forgetting_rate,
    head_norm_gain,
    output_weight,
    feedforward_norm_gain,
    gate_weight,
    up_weight,
    down_weight,
):
    tokens = queries.shape[0]
    owned_heads = queries.shape[1] // HK
    blocks = tokens // BLOCK
    forgetting_exponent = (
        jax.nn.log_sigmoid(forgetting_raw_score) / sigmoid_sharpness + additional_forgetting_rate
    )
    query_part = split_heads(queries, blocks, owned_heads, HK) * HK ** (-0.5)
    key_part = split_heads(key_matrix, blocks, owned_heads, HK)
    value_part = split_heads(value_matrix, blocks, owned_heads, HV)
    decay_part = split_heads(forgetting_exponent, blocks, owned_heads, HK)
    within = jnp.cumsum(decay_part, axis=2)
    closing = within[:, :, -1, :]
    query_in = query_part * jnp.exp(within)
    key_in = key_part * jnp.exp(-within)
    key_end = key_part * jnp.exp(closing[:, :, None, :] - within)
    causal = jnp.tril(jnp.ones((BLOCK, BLOCK), jnp.bool_))
    scores = jnp.einsum("hntd,hnsd->hnts", query_in, key_in, precision=highest)
    scores = jnp.where(causal, scores, 0.0)
    inside = jnp.einsum("hnts,hnsv->hntv", scores, value_part, precision=highest)

    def advance(memory, inputs):
        query_block, key_block, value_block, decay_block = inputs
        final_answer = jnp.einsum("htd,hdv->htv", query_block, memory, precision=highest)
        memory = decay_block[:, :, None] * memory + jnp.einsum(
            "hsd,hsv->hdv", key_block, value_block, precision=highest
        )
        return (memory, final_answer)

    sequence = (
        jnp.moveaxis(query_in, 1, 0),
        jnp.moveaxis(key_end, 1, 0),
        jnp.moveaxis(value_part, 1, 0),
        jnp.moveaxis(jnp.exp(closing), 1, 0),
    )
    start_memory = jnp.zeros((owned_heads, HK, HV), jnp.float32)
    final_memory, earlier_blocks = lax.scan(advance, start_memory, sequence)
    device_decay = jnp.exp(jnp.sum(closing, axis=1))
    neutral = (jnp.ones_like(device_decay), jnp.zeros_like(final_memory))
    _, carried = carried_in((device_decay, final_memory), "sp", combine, neutral)
    before = jnp.cumsum(closing, axis=1) - closing
    query_far = query_in * jnp.exp(before[:, :, None, :])
    outside = jnp.einsum("hntd,hdv->hntv", query_far, carried, precision=highest)
    mixed_heads = inside + jnp.moveaxis(earlier_blocks, 0, 1) + outside
    mixed_heads = mixed_heads.transpose(1, 2, 0, 3).reshape(tokens, owned_heads, HV)
    mixed_heads = mixed_heads * lax.rsqrt(
        jnp.mean(mixed_heads * mixed_heads, axis=-1, keepdims=True) + epsilon
    )
    gated_rows = (
        mixed_heads.reshape(tokens, owned_heads * HV)
        * head_norm_gain
        * jax.nn.silu(output_gate_logits.astype(jnp.float32))
    ).astype(jnp.bfloat16)
    partial_out = jnp.dot(gated_rows, output_weight, preferred_element_type=jnp.float32)
    model_width = stream.shape[1]
    column_share = model_width // lax.axis_size("tp")
    column_start = lax.axis_index("tp") * column_share
    attn_cols = lax.psum_scatter(
        partial_out.astype(jnp.bfloat16), "tp", scatter_dimension=1, tiled=True
    ).astype(jnp.float32)
    resid_part = (
        lax.dynamic_slice_in_dim(stream, column_start, column_share, 1).astype(jnp.float32)
        + attn_cols
    )
    elementwise_power = lax.psum(jnp.sum(resid_part * resid_part, axis=1), "tp")
    gain_part = lax.dynamic_slice_in_dim(
        feedforward_norm_gain, column_start, column_share, 0
    ).astype(jnp.float32)
    rescaled_portion = (
        resid_part * lax.rsqrt(elementwise_power / model_width + epsilon)[:, None] * gain_part
    ).astype(jnp.bfloat16)
    normed = lax.all_gather(rescaled_portion, "tp", axis=1, tiled=True)
    gate_sum = jnp.dot(
        normed,
        lax.all_gather(gate_weight, "sp", axis=0, tiled=True),
        preferred_element_type=jnp.float32,
    )
    up_sum = jnp.dot(
        normed,
        lax.all_gather(up_weight, "sp", axis=0, tiled=True),
        preferred_element_type=jnp.float32,
    )
    hidden = (jax.nn.silu(gate_sum) * up_sum).astype(jnp.bfloat16)
    down_sum = jnp.dot(
        hidden,
        lax.all_gather(down_weight, "sp", axis=1, tiled=True),
        preferred_element_type=jnp.float32,
    )
    ffn_part = lax.psum_scatter(
        down_sum.astype(jnp.bfloat16), "tp", scatter_dimension=1, tiled=True
    ).astype(jnp.float32)
    return (resid_part + ffn_part).astype(jnp.bfloat16)


def solution(mesh):
    return jax.shard_map(
        local,
        mesh=mesh,
        in_specs=(
            P(("grp", "sp"), None),
            P(("grp", "sp"), "tp"),
            P(("grp", "sp"), "tp"),
            P(("grp", "sp"), "tp"),
            P(("grp", "sp"), "tp"),
            P(("grp", "sp"), "tp"),
            P(("grp", "sp"), "tp"),
            P("tp"),
            P("tp", None),
            P(),
            P("sp", "tp"),
            P("sp", "tp"),
            P("tp", "sp"),
        ),
        out_specs=P(("grp", "sp"), "tp"),
        check_vma=False,
    )
```

profile of v0, /device:TPU:0, one launch (start us, length us, event | category | flops | bytes accessed | tf_op | source)
XLA Modules:
  0.0 430.0 jit_solution(5797290989619579910)
XLA Ops:
  6.5 1.2 fusion.27
  8.0 0.9 convert_element_type.88
  8.9 0.9 convert.4
  9.8 1.5 bitcast_multiply_fusion.1
  11.4 3.6 while.26
  11.4 1.1 fusion.60
  13.2 1.1 fusion.60
  15.8 12.6 %all-gather.2 = bf16[4,1,256]{2,1,0:T(2,128)(2,1)S(1)} all-gather(bf16[1,1,256]{2,1,0:T(2,128)(2,1)S(1)} %reshape.243), channel_id=2, replica_groups=mesh['grp'=2,'sp'=4,'tp'=4] {'sp'}, dimensions={0}, use_global_device_ids=true | all-gather | bytes 2560 | tf_op jit(solution)/shard_map/all_gather | solution.py:17
  28.8 1.3 convolution_add_fusion.1
  30.1 16.3 %all-gather.14.cloned.1.call-done = bf16[4,256,512]{2,1,0:T(8,128)(2,1)} async-done(((bf16[1,256,512]{2,1,0:T(8,128)(2,1)}), bf16[4,256,512]{2,1,0:T(8,128)(2,1)}) %all-gather.14.cloned.1.call-update) | async-done | bytes 1048592 | tf_op jit(solution)/shard_map/all_gather | solution.py:17
  47.2 1.2 convolution_convert_fusion
  50.5 0.8 dynamic-slice_convert_fusion.1
  51.2 22.1 %reduce-scatter.3.cloned.1.call-done = bf16[128,512]{1,0:T(8,128)(2,1)} async-done(((bf16[128,2048]{1,0:T(8,128)(2,1)}), bf16[128,512]{1,0:T(8,128)(2,1)}) %reduce-scatter.3.cloned.1.call-update) | async-done | bytes 131088 | tf_op jit(solution)/shard_map/reduce_scatter | solution.py:113
  73.3 1.1 multiply_reduce_fusion
  74.4 5.8 %psum.7 = f32[128]{0:T(128)S(1)} all-reduce(f32[128]{0:T(128)S(1)} %multiply_reduce_fusion), channel_id=1, replica_groups=mesh['grp'=2,'sp'=4,'tp'=4] {'tp'}, use_global_device_ids=true, to_apply=%region_10.11 | all-reduce | flops 128 | bytes 1024 | tf_op jit(solution)/shard_map/psum | solution.py:120
  80.2 1.1 multiply_convert_fusion
  81.2 6.9 %all_gather.25 = bf16[128,2048]{1,0:T(8,128)(2,1)S(1)} all-gather(bf16[128,512]{1,0:T(8,128)(2,1)S(1)} %multiply_convert_fusion), channel_id=1, replica_groups=mesh['grp'=2,'sp'=4,'tp'=4] {'tp'}, dimensions={1}, use_global_device_ids=true | all-gather | bytes 655360 | tf_op jit(solution)/shard_map/all_gather | solution.py:127
  88.1 93.5 %all-gather.8.cloned.1.call-done = bf16[2048,1408]{1,0:T(8,128)(2,1)} async-done(((bf16[512,1408]{1,0:T(8,128)(2,1)}), bf16[2048,1408]{1,0:T(8,128)(2,1)}) %all-gather.8.cloned.1.call-update) | async-done | bytes 5767184 | tf_op jit(solution)/shard_map/all_gather | solution.py:130
  181.6 3.6 fusion.38
  185.3 102.8 %all-gather.10.cloned.1.call-done = bf16[2048,1408]{1,0:T(8,128)(2,1)} async-done(((bf16[512,1408]{1,0:T(8,128)(2,1)}), bf16[2048,1408]{1,0:T(8,128)(2,1)}) %all-gather.10.cloned.1.call-update) | async-done | bytes 5767184 | tf_op jit(solution)/shard_map/all_gather | solution.py:135
  288.0 106.4 %all-gather.12.cloned.1.call-done = bf16[1408,2048]{1,0:T(8,128)(2,1)} async-done(((bf16[1408,512]{1,0:T(8,128)(2,1)}), bf16[1408,2048]{1,0:T(8,128)(2,1)}) %all-gather.12.cloned.1.call-update) | async-done | bytes 5767184 | tf_op jit(solution)/shard_map/all_gather | solution.py:141
  394.4 7.0 %convolution_convert_fusion.1 = bf16[128,2048]{1,0:T(8,128)(2,1)} fusion(bf16[1408,2048]{1,0:T(8,128)(2,1)} %all-gather.12.cloned.1.call-done, bf16[128,2048]{1,0:T(8,128)(2,1)S(1)} %all_gather.25, bf16[2048,1408]{1,0:T(8,128)(2,1)} %all-gather.10.cloned.1.call-done, f32[128,1408]{1,0:T(8,128)S(1)} %fusion.38), kind=kOutput, calls=%fused_computation.23 | convolution fusion | flops 1477738496 | bytes 13303808 | tf_op jit(solution)/shard_map/dot_general | solution.py:139
  401.5 20.0 %reduce-scatter.5.cloned.1.call-done = bf16[128,512]{1,0:T(8,128)(2,1)} async-done(((bf16[128,2048]{1,0:T(8,128)(2,1)}), bf16[128,512]{1,0:T(8,128)(2,1)}) %reduce-scatter.5.cloned.1.call-update) | async-done | bytes 131088 | tf_op jit(solution)/shard_map/reduce_scatter | solution.py:144
  421.5 1.7 add_convert_fusion
  (47 shorter events, 5.5 us)
Async XLA Ops:
  6.5 40.7 %copy-start = (bf16[512,2048]{1,0:T(8,128)(2,1)S(1)}, bf16[512,2048]{1,0:T(8,128)(2,1)}, u32[]{:S(2)}) copy-start(bf16[512,2048]{1,0:T(8,128)(2,1)} %param.25) | copy-start | bytes 6291460
  6.5 39.9 %all-gather.14.cloned.1.call-start = ((), (), s32[]{:S(2)}) async-start(), calls=%async_computation.7 | async-start | bytes 1310720 | tf_op jit(solution)/shard_map/all_gather | solution.py:17
  15.0 32.1 %copy-start.4 = (f32[512]{0:T(512)S(1)}, f32[512]{0:T(512)}, u32[]{:S(2)}) copy-start(f32[512]{0:T(512)} %param.24) | copy-start | bytes 6148
  15.7 57.6 %reduce-scatter.3.cloned.1.call-start = ((), (), s32[]{:S(2)}) async-start(), calls=%async_computation.2 | async-start | bytes 655360 | tf_op jit(solution)/shard_map/reduce_scatter | solution.py:113
  28.8 17.7 %copy-start.2 = (f32[128,256]{1,0:T(8,128)S(1)}, f32[128,256]{1,0:T(8,128)}, u32[]{:S(2)}) copy-start(f32[128,256]{1,0:T(8,128)} %get-tuple-element.167) | copy-start | bytes 393220
  28.8 18.3 %copy-start.3 = (bf16[128,512]{1,0:T(8,128)(2,1)S(1)}, bf16[128,512]{1,0:T(8,128)(2,1)}, u32[]{:S(2)}) copy-start(bf16[128,512]{1,0:T(8,128)(2,1)} %param.21) | copy-start | bytes 393220
  48.5 133.1 %all-gather.8.cloned.1.call-start = ((), (), s32[]{:S(2)}) async-start(), calls=%async_computation.3 | async-start | bytes 7208960 | tf_op jit(solution)/shard_map/all_gather | solution.py:130
  49.2 238.8 %all-gather.10.cloned.1.call-start = ((), (), s32[]{:S(2)}) async-start(), calls=%async_computation.4 | async-start | bytes 7208960 | tf_op jit(solution)/shard_map/all_gather | solution.py:135
  49.8 344.6 %all-gather.12.cloned.1.call-start = ((), (), s32[]{:S(2)}) async-start(), calls=%async_computation.5 | async-start | bytes 7208960 | tf_op jit(solution)/shard_map/all_gather | solution.py:141
  50.4 371.1 %reduce-scatter.5.cloned.1.call-start = ((), (), s32[]{:S(2)}) async-start(), calls=%async_computation.6 | async-start | bytes 655360 | tf_op jit(solution)/shard_map/reduce_scatter | solution.py:144
  185.3 236.3 %copy-start.1 = (bf16[128,512]{1,0:T(8,128)(2,1)S(1)}, bf16[128,512]{1,0:T(8,128)(2,1)}, u32[]{:S(2)}) copy-start(bf16[128,512]{1,0:T(8,128)(2,1)} %reduce-scatter.3.cloned.1.call-done) | copy-start | bytes 393220
Sparse Core Ops, SparseCore 0:
  15.9 30.5 all-gather.13
  48.9 24.3 reduce-scatter.2
  74.9 106.6 all-gather.7
  183.1 104.9 all-gather.9
  289.4 104.9 all-gather.11
  401.6 19.8 reduce-scatter.4
where the time goes:
time: 431 us; the launch traced here: 430 us
  waiting for transfers between devices  363 us (84%)
  blocking collectives  25.3 us (6%)
  matrix products  17.6 us (4%)
  between operations  13.7 us (3%)
  other arithmetic  10.2 us (2%)
    all_gather x1, waiting for transfers between devices, local(): lax.all_gather(down_weight, 'sp', axis=1, tiled=True)  106 us
    all_gather x1, waiting for transfers between devices, local(): lax.all_gather(up_weight, 'sp', axis=0, tiled=True)  103 us
    all_gather x1, waiting for transfers between devices, local(): lax.all_gather(gate_weight, 'sp', axis=0, tiled=True)  93.5 us
    reduce_scatter x1, waiting for transfers between devices, local(): lax.psum_scatter(partial_out.astype(jnp.bfloat16), 'tp', scatter_dimensio...  22.1 us
    reduce_scatter x1, waiting for transfers between devices, local(): lax.psum_scatter(down_sum.astype(jnp.bfloat16), 'tp', scatter_dimension=1...  20 us
    all_gather x1, waiting for transfers between devices, carried_in(): lax.all_gather(a.astype(kind), axis)  16.3 us
    all_gather x1, blocking collectives, carried_in(): lax.all_gather(a.astype(kind), axis)  12.6 us
  transfers between devices with their start and end apart: 6, of which 6 were waited for; matrix products, arithmetic and copies ran while one was open for 2% of the time, Pallas kernels for 0%

commit v1 on v0

--- a/solution.py
+++ b/solution.py
@@ -54,6 +54,30 @@
     up_weight,
     down_weight,
 ):
+
+    def fix_routes_all(xx, dim_i):
+        res = lax.axis_size("sp")
+        a_next, after, near = (res, lax.axis_index("sp"), xx.shape[dim_i])
+        inbox = [u * a_next if to_i == dim_i else u for to_i, u in enumerate(xx.shape)]
+        formed = jnp.zeros(inbox, xx.dtype)
+        e_next = lax.dynamic_update_slice_in_dim(formed, xx, after * near, axis=dim_i)
+        right_arr = z1 = xx
+        dev_j = 1
+        while dev_j < a_next // 2 + 1:
+            right_arr = lax.ppermute(
+                right_arr, "sp", [(to_i, (to_i + 1) % a_next) for to_i in range(a_next)]
+            )
+            e_next = lax.dynamic_update_slice_in_dim(
+                e_next, right_arr, (after - dev_j) % a_next * near, axis=dim_i
+            )
+            if 2 * dev_j < a_next:
+                z1 = lax.ppermute(z1, "sp", [(to_i, (to_i - 1) % a_next) for to_i in range(a_next)])
+                e_next = lax.dynamic_update_slice_in_dim(
+                    e_next, z1, (after + dev_j) % a_next * near, axis=dim_i
+                )
+            dev_j = dev_j + 1
+        return e_next
+
     tokens = queries.shape[0]
     owned_heads = queries.shape[1] // HK
     blocks = tokens // BLOCK
@@ -136,11 +160,7 @@
         preferred_element_type=jnp.float32,
     )
     hidden = (jax.nn.silu(gate_sum) * up_sum).astype(jnp.bfloat16)
-    down_sum = jnp.dot(
-        hidden,
-        lax.all_gather(down_weight, "sp", axis=1, tiled=True),
-        preferred_element_type=jnp.float32,
-    )
+    down_sum = jnp.dot(hidden, fix_routes_all(down_weight, 1), preferred_element_type=jnp.float32)
     ffn_part = lax.psum_scatter(
         down_sum.astype(jnp.bfloat16), "tp", scatter_dimension=1, tiled=True
     ).astype(jnp.float32)

time: 431 us -> 386 us (0.90)
  waiting for transfers between devices: 363 us -> 287 us
  starting transfers between devices: 0.2 us -> 17.7 us
  local copies, waits for them, and re-layouts: 0.2 us -> 14 us
    ppermute x0 -> x3, waiting for transfers between devices: none -> 130 us  [the longest x1 103 us: fix_routes_all(): lax.ppermute(z1, 'sp', [(to_i, (to_i - 1) % a_next) for to_i in range(a_n...]
    all_gather x1 -> x0, waiting for transfers between devices: 106 us -> none  [local(): lax.all_gather(down_weight, 'sp', axis=1, tiled=True)]
    all_gather x1, waiting for transfers between devices: 93.5 us -> 15.5 us  [local(): lax.all_gather(gate_weight, 'sp', axis=0, tiled=True)]
    reduce_scatter x1, waiting for transfers between devices: 22.1 us -> 0.01 us  [local(): lax.psum_scatter(partial_out.astype(jnp.bfloat16), 'tp', scatter_dimensio...]
    ppermute x0 -> x3, starting transfers between devices: none -> 17.6 us  [the longest x2 14.9 us: fix_routes_all(): lax.ppermute(right_arr, 'sp', [(to_i, (to_i + 1) % a_next) for to_i in ra...]
    dynamic_update_slice x0 -> x4, local copies, waits for them, and re-layouts: none -> 10.6 us  [the longest x2 5.27 us: fix_routes_all(): lax.dynamic_update_slice_in_dim(e_next, right_arr, (after - dev_j) % a_ne...]
  transfers between devices with their start and end apart: 6 -> 8, of which waited for: 6 -> 6; matrix products, arithmetic and copies ran while one was open for 2% -> 6% of each run, Pallas kernels for 0% -> 0%
where the time goes in v1:
time: 386 us; the launch traced here: 385 us
  waiting for transfers between devices  287 us (74%)
  blocking collectives  25.2 us (7%)
  starting transfers between devices  17.7 us (5%)
  matrix products  17.6 us (5%)
  local copies, waits for them, and re-layouts  14 us (4%)
  between operations  13.3 us (3%)
  other arithmetic  10.1 us (3%)
    all_gather x1, waiting for transfers between devices, local(): lax.all_gather(up_weight, 'sp', axis=0, tiled=True)  104 us
    ppermute x1, waiting for transfers between devices, fix_routes_all(): lax.ppermute(z1, 'sp', [(to_i, (to_i - 1) % a_next) for to_i in range(a_n...  103 us
    ppermute x2, waiting for transfers between devices, fix_routes_all(): lax.ppermute(right_arr, 'sp', [(to_i, (to_i + 1) % a_next) for to_i in ra...  26.9 us
    reduce_scatter x1, waiting for transfers between devices, local(): lax.psum_scatter(down_sum.astype(jnp.bfloat16), 'tp', scatter_dimension=1...  20 us
    all_gather x1, waiting for transfers between devices, carried_in(): lax.all_gather(a.astype(kind), axis)  16.3 us
    all_gather x1, waiting for transfers between devices, local(): lax.all_gather(gate_weight, 'sp', axis=0, tiled=True)  15.5 us
    ppermute x2, starting transfers between devices, fix_routes_all(): lax.ppermute(right_arr, 'sp', [(to_i, (to_i + 1) % a_next) for to_i in ra...  14.9 us
    all_gather x1, blocking collectives, carried_in(): lax.all_gather(a.astype(kind), axis)  12.7 us
  transfers between devices with their start and end apart: 8, of which 6 were waited for; matrix products, arithmetic and copies ran while one was open for 6% of the time, Pallas kernels for 0%

profile of v1, /device:TPU:0, one launch (start us, length us, event | category | flops | bytes accessed | tf_op | source)
XLA Modules:
  0.0 384.9 jit_solution(11153360449179475537)
XLA Ops:
  9.8 1.5 bitcast_multiply_fusion.1
  11.4 3.6 while.26
  15.9 12.7 %all-gather.2 = bf16[4,1,256]{2,1,0:T(2,128)(2,1)S(1)} all-gather(bf16[1,1,256]{2,1,0:T(2,128)(2,1)S(1)} %reshape.243), channel_id=2, replica_groups=mesh['grp'=2,'sp'=4,'tp'=4] {'sp'}, dimensions={0}, use_global_device_ids=true | all-gather | bytes 2560 | tf_op jit(solution)/shard_map/all_gather | solution.py:17
  28.8 1.3 convolution_add_fusion.1
  30.2 16.3 %all-gather.11.cloned.1.call-done = bf16[4,256,512]{2,1,0:T(8,128)(2,1)} async-done(((bf16[1,256,512]{2,1,0:T(8,128)(2,1)}), bf16[4,256,512]{2,1,0:T(8,128)(2,1)}) %all-gather.11.cloned.1.call-update) | async-done | bytes 1048592 | tf_op jit(solution)/shard_map/all_gather | solution.py:17
  47.3 1.3 convolution_convert_fusion
  49.9 2.8 collective-permute-start
  52.8 2.7 collective-permute-start.1
  55.5 3.2 broadcast_in_dim.33
  58.7 2.7 constant_dynamic-update-slice_fusion.3
  61.3 26.9 %collective-permute-done = bf16[1408,512]{1,0:T(8,128)(2,1)} collective-permute-done((bf16[1408,512]{1,0:T(8,128)(2,1)}, bf16[1408,512]{1,0:T(8,128)(2,1)}, u32[]{:S(2)}, u32[]{:S(2)}) %collective-permute-start) | collective-permute-done | bytes 1441824 | tf_op jit(solution)/shard_map/ppermute | solution.py:67
  88.2 12.0 %collective-permute-start.2 = (bf16[1408,512]{1,0:T(8,128)(2,1)}, bf16[1408,512]{1,0:T(8,128)(2,1)}, u32[]{:S(2)}, u32[]{:S(2)}) collective-permute-start(bf16[1408,512]{1,0:T(8,128)(2,1)} %collective-permute-done), channel_id=1, source_target_pairs={{0,4},{4,8},{8,12},{12,0},{1,5},{5,9},{9,13},{13,1},{2,6},{6,10},{... | collective-permute-start | bytes 4325384 | tf_op jit(solution)/shard_map/ppermute | solution.py:67
  101.0 2.6 constant_dynamic-update-slice_fusion.2
  103.6 103.0 %collective-permute-done.1 = bf16[1408,512]{1,0:T(8,128)(2,1)} collective-permute-done((bf16[1408,512]{1,0:T(8,128)(2,1)}, bf16[1408,512]{1,0:T(8,128)(2,1)}, u32[]{:S(2)}, u32[]{:S(2)}) %collective-permute-start.1) | collective-permute-done | bytes 1441824 | tf_op jit(solution)/shard_map/ppermute | solution.py:74
  206.7 2.6 constant_dynamic-update-slice_fusion.1
  210.3 6.1 %psum.7 = f32[128]{0:T(128)S(1)} all-reduce(f32[128]{0:T(128)S(1)} %multiply_reduce_fusion), channel_id=1, replica_groups=mesh['grp'=2,'sp'=4,'tp'=4] {'tp'}, use_global_device_ids=true, to_apply=%region_10.11 | all-reduce | flops 128 | bytes 1024 | tf_op jit(solution)/shard_map/psum | solution.py:144
  217.4 6.5 %all_gather.22 = bf16[128,2048]{1,0:T(8,128)(2,1)S(1)} all-gather(bf16[128,512]{1,0:T(8,128)(2,1)S(1)} %multiply_convert_fusion), channel_id=1, replica_groups=mesh['grp'=2,'sp'=4,'tp'=4] {'tp'}, dimensions={1}, use_global_device_ids=true | all-gather | bytes 655360 | tf_op jit(solution)/shard_map/all_gather | solution.py:151
  223.9 2.6 constant_dynamic-update-slice_fusion
  226.5 15.5 %all-gather.7.cloned.1.call-done = bf16[2048,1408]{1,0:T(8,128)(2,1)} async-done(((bf16[512,1408]{1,0:T(8,128)(2,1)}), bf16[2048,1408]{1,0:T(8,128)(2,1)}) %all-gather.7.cloned.1.call-update) | async-done | bytes 5767184 | tf_op jit(solution)/shard_map/all_gather | solution.py:154
  242.0 3.6 fusion.38
  245.7 103.9 %all-gather.9.cloned.1.call-done = bf16[2048,1408]{1,0:T(8,128)(2,1)} async-done(((bf16[512,1408]{1,0:T(8,128)(2,1)}), bf16[2048,1408]{1,0:T(8,128)(2,1)}) %all-gather.9.cloned.1.call-update) | async-done | bytes 5767184 | tf_op jit(solution)/shard_map/all_gather | solution.py:159
  349.6 7.0 %convolution_convert_fusion.1 = bf16[128,2048]{1,0:T(8,128)(2,1)} fusion(bf16[1408,2048]{1,0:T(8,128)(2,1)} %constant_dynamic-update-slice_fusion, bf16[128,2048]{1,0:T(8,128)(2,1)S(1)} %all_gather.22, bf16[2048,1408]{1,0:T(8,128)(2,1)} %all-gather.9.cloned.1.call-done, f32[128,1408]{1,0:T(8,128)S(1)} %fusion.38), kind=kOutput, calls=%fused_computation.23 | convolution fusion | flops 1477738496 | bytes 13303808 | tf_op jit(solution)/shard_map/dot_general | solution.py:163
  356.7 20.0 %reduce-scatter.5.cloned.1.call-done = bf16[128,512]{1,0:T(8,128)(2,1)} async-done(((bf16[128,2048]{1,0:T(8,128)(2,1)}), bf16[128,512]{1,0:T(8,128)(2,1)}) %reduce-scatter.5.cloned.1.call-update) | async-done | bytes 131088 | tf_op jit(solution)/shard_map/reduce_scatter | solution.py:164
  376.7 1.7 add_convert_fusion
  (57 shorter events, 12.9 us)
Async XLA Ops:
  6.5 40.7 %copy-start = (bf16[512,2048]{1,0:T(8,128)(2,1)S(1)}, bf16[512,2048]{1,0:T(8,128)(2,1)}, u32[]{:S(2)}) copy-start(bf16[512,2048]{1,0:T(8,128)(2,1)} %param.25) | copy-start | bytes 6291460
  6.5 39.9 %all-gather.11.cloned.1.call-start = ((), (), s32[]{:S(2)}) async-start(), calls=%async_computation.6 | async-start | bytes 1310720 | tf_op jit(solution)/shard_map/all_gather | solution.py:17
  15.0 32.1 %copy-start.5 = (f32[512]{0:T(512)S(1)}, f32[512]{0:T(512)}, u32[]{:S(2)}) copy-start(f32[512]{0:T(512)} %param.24) | copy-start | bytes 6148
  15.8 193.5 %reduce-scatter.3.cloned.1.call-start = ((), (), s32[]{:S(2)}) async-start(), calls=%async_computation.2 | async-start | bytes 655360 | tf_op jit(solution)/shard_map/reduce_scatter | solution.py:137
  28.8 17.7 %copy-start.2 = (f32[128,256]{1,0:T(8,128)S(1)}, f32[128,256]{1,0:T(8,128)}, u32[]{:S(2)}) copy-start(f32[128,256]{1,0:T(8,128)} %get-tuple-element.167) | copy-start | bytes 393220
  28.8 18.3 %copy-start.4 = (bf16[128,512]{1,0:T(8,128)(2,1)S(1)}, bf16[128,512]{1,0:T(8,128)(2,1)}, u32[]{:S(2)}) copy-start(bf16[128,512]{1,0:T(8,128)(2,1)} %param.21) | copy-start | bytes 393220
  48.6 193.5 %all-gather.7.cloned.1.call-start = ((), (), s32[]{:S(2)}) async-start(), calls=%async_computation.3 | async-start | bytes 7208960 | tf_op jit(solution)/shard_map/all_gather | solution.py:154
  49.3 300.3 %all-gather.9.cloned.1.call-start = ((), (), s32[]{:S(2)}) async-start(), calls=%async_computation.4 | async-start | bytes 7208960 | tf_op jit(solution)/shard_map/all_gather | solution.py:159
  49.9 326.9 %reduce-scatter.5.cloned.1.call-start = ((), (), s32[]{:S(2)}) async-start(), calls=%async_computation.5 | async-start | bytes 655360 | tf_op jit(solution)/shard_map/reduce_scatter | solution.py:164
  49.9 38.3 %collective-permute-start = (bf16[1408,512]{1,0:T(8,128)(2,1)}, bf16[1408,512]{1,0:T(8,128)(2,1)}, u32[]{:S(2)}, u32[]{:S(2)}) collective-permute-start(bf16[1408,512]{1,0:T(8,128)(2,1)} %param.29), channel_id=1, source_target_pairs={{0,4},{4,8},{8,12},{12,0},{1,5},{5,9},{9,13},{13,1},{2,6},{6,10},{... | collective-permute-start | bytes 4325384 | tf_op jit(solution)/shard_map/ppermute | solution.py:67
  52.8 153.9 %collective-permute-start.1 = (bf16[1408,512]{1,0:T(8,128)(2,1)}, bf16[1408,512]{1,0:T(8,128)(2,1)}, u32[]{:S(2)}, u32[]{:S(2)}) collective-permute-start(bf16[1408,512]{1,0:T(8,128)(2,1)} %param.29), channel_id=1, source_target_pairs={{0,12},{4,0},{8,4},{12,8},{1,13},{5,1},{9,5},{13,9},{2,14},{6,2},{... | collective-permute-start | bytes 4325384 | tf_op jit(solution)/shard_map/ppermute | solution.py:74
  58.7 150.6 %copy-start.3 = (bf16[128,2048]{1,0:T(8,128)(2,1)S(1)}, bf16[128,2048]{1,0:T(8,128)(2,1)}, u32[]{:S(2)}) copy-start(bf16[128,2048]{1,0:T(8,128)(2,1)} %param.17) | copy-start | bytes 1572868
  88.2 135.7 %collective-permute-start.2 = (bf16[1408,512]{1,0:T(8,128)(2,1)}, bf16[1408,512]{1,0:T(8,128)(2,1)}, u32[]{:S(2)}, u32[]{:S(2)}) collective-permute-start(bf16[1408,512]{1,0:T(8,128)(2,1)} %collective-permute-done), channel_id=1, source_target_pairs={{0,4},{4,8},{8,12},{12,0},{1,5},{5,9},{9,13},{13,1},{2,6},{6,10},{... | collective-permute-start | bytes 4325384 | tf_op jit(solution)/shard_map/ppermute | solution.py:67
  245.7 131.1 %copy-start.1 = (bf16[128,512]{1,0:T(8,128)(2,1)S(1)}, bf16[128,512]{1,0:T(8,128)(2,1)}, u32[]{:S(2)}) copy-start(bf16[128,512]{1,0:T(8,128)(2,1)} %reduce-scatter.3.cloned.1.call-done) | copy-start | bytes 393220
Sparse Core Ops, SparseCore 0:
  15.9 30.5 all-gather.10
  48.9 24.3 reduce-scatter.2
  74.9 167.0 all-gather.6
  243.5 106.0 all-gather.8
  356.8 19.8 reduce-scatter.4
